TPU v7x, 512 devices: a whole 4x4x16 slice. The times are simulated.
512 devices in a mesh: ep: 32 (over z, core), tp: 16 (over y, x).
Axes of the slice: x: 4, y: 4, z: 16, core: 2. Of those that a mesh axis runs over, the one named last changes fastest.
Arguments:
- query_rows: bfloat16 [24576, 1024], P('ep', 'tp'), may hold values from -600 to 600
- key_rows: bfloat16 [24576, 1024], P('ep', 'tp'), may hold values from -6 to 6
- value_rows: bfloat16 [24576, 1024], P('ep', 'tp'), may hold values from -6 to 6
- cum_gate: float32 [16, 24576], P('tp'), may hold values from -2458 to 0, as said below
- out_weight: bfloat16 [1024, 2048], P(None, 'tp'), may hold values from -0.1875 to 0.1875
- moe_input: bfloat16 [6144, 2048], P('ep'), may hold values from -6 to 6
- moe_gain: float32 [2048], replicated, may hold values from 0.1 to 1.9
- routes: int32 [6144, 3], P('ep'), may hold values from 0 to 127, all different within a row; in each aligned block of 192 rows (0 to 191, 192 to 383, ...) at most 9 rows name the same one
- route_weight: float32 [6144, 3], P('ep'), may hold values from 0.2 to 1.5
- expert_gate: bfloat16 [128, 2048, 512], P('ep', None, 'tp'), may hold values from -0.125 to 0.125
- expert_up: bfloat16 [128, 2048, 512], P('ep', None, 'tp'), may hold values from -0.125 to 0.125
- expert_down: bfloat16 [128, 512, 2048], P('ep', None, 'tp'), may hold values from -0.25 to 0.25
- shared_gate: bfloat16 [2048, 512], P(None, 'tp'), may hold values from -0.125 to 0.125
- shared_up: bfloat16 [2048, 512], P(None, 'tp'), may hold values from -0.125 to 0.125
- shared_down: bfloat16 [512, 2048], P(None, 'tp'), may hold values from -0.25 to 0.25
Outputs:
- mixer_out: bfloat16 [24576, 2048], P('ep', 'tp')
- moe_out: bfloat16 [6144, 2048], P('ep', 'tp')
Inputs may be any that keep to these rules, and one draw needn't show every extreme that they name: Non-increasing along positions: cum_gate[h, t] is the sum of the log forget gates of head h over positions 0 to t. `routes`: the 3 experts of a token differ. In each aligned block of 192 tokens no expert is named by more than 9 tokens, a bound that some block reaches.
All inputs are finite; a program needn't handle non-finite values.
Results may differ from a plain program's by a relative error of at most 0.0068.
Values may be sent and summed in bfloat16 or wider, within the bound.
No kernel may reach another device: no remote copies, remote signals or barrier semaphores. Data moves between devices by JAX's collectives and lax.ppermute only.
A program may use at most 64 MiB of HBM per device.

v0:
```python
import jax
import jax.numpy as jnp
from jax import lax
from jax.sharding import PartitionSpec as P

HEAD = 64
neg_fill = -1e30
norm_eps = 1e-06


def joined_along(pieces, dim):
    dims = list(pieces.shape[1:])
    dims[dim] *= pieces.shape[0]
    return jnp.moveaxis(pieces, 0, dim).reshape(dims)


def sent_to_all(array, axis):
    copies = jnp.broadcast_to(array, (lax.axis_size(axis), *array.shape))
    return lax.all_to_all(copies, axis, split_axis=0, concat_axis=0, tiled=True)


def collect(array, axis, dim):
    return joined_along(sent_to_all(array, axis), dim)


def local(
    query_rows,
    key_rows,
    value_rows,
    cum_gate,
    out_weight,
    moe_input,
    moe_gain,
    routes,
    route_weight,
    expert_gate,
    expert_up,
    expert_down,
    shared_gate,
    shared_up,
    shared_down,
):
    row_count = query_rows.shape[0]
    width = query_rows.shape[1]
    local_heads = width // HEAD
    scale = HEAD ** (-0.5)
    first_row = lax.axis_index("ep") * row_count
    last_row = first_row + row_count - 1
    query_heads = query_rows.reshape(row_count, local_heads, HEAD)
    query_gate = lax.dynamic_slice_in_dim(cum_gate, first_row, row_count, 1)
    query_pos = first_row + jnp.arange(row_count, dtype=jnp.int32)
    key_value = jnp.concatenate([key_rows, value_rows], axis=1)
    initial = (
        jnp.full((local_heads, row_count), neg_fill, jnp.float32),
        jnp.zeros((local_heads, row_count), jnp.float32),
        jnp.zeros((local_heads, row_count, HEAD), jnp.float32),
    )
    shard_rows = lax.all_gather(key_value, "ep", axis=0, tiled=True)
    piece_len = shard_rows.shape[0]
    key_span = 512

    def one_span(state_in, span_index):
        span_start = span_index * key_span

        def update(state_old):
            running_max, denominator, weighted = state_old
            block = lax.dynamic_slice_in_dim(shard_rows, span_index * key_span, key_span, 0)
            keys_block = block[:, :width].reshape(key_span, local_heads, HEAD)
            values_block = block[:, width:].reshape(key_span, local_heads, HEAD)
            key_gate = lax.dynamic_slice_in_dim(cum_gate, span_start, key_span, 1)
            scores = (
                jnp.einsum(
                    "qhd,khd->hqk", query_heads, keys_block, preferred_element_type=jnp.float32
                )
                * scale
            )
            scores = scores + query_gate[:, :, None] - key_gate[:, None, :]
            causal = (span_start + jnp.arange(key_span, dtype=jnp.int32))[None, :] <= query_pos[
                :, None
            ]
            scores = jnp.where(causal[None], scores, neg_fill)
            new_max = jnp.maximum(running_max, jnp.max(scores, axis=2))
            expon = jnp.where(causal[None], jnp.exp(scores - new_max[:, :, None]), 0.0)
            rescale = jnp.exp(running_max - new_max)
            denominator = denominator * rescale + jnp.sum(expon, axis=2)
            weighted = weighted * rescale[:, :, None] + jnp.einsum(
                "hqk,khd->hqd",
                expon.astype(jnp.bfloat16),
                values_block,
                preferred_element_type=jnp.float32,
            )
            return (new_max, denominator, weighted)

        state_next = lax.cond(span_start <= last_row, update, lambda unchanged: unchanged, state_in)
        return (state_next, None)

    state_out, _ = lax.scan(one_span, initial, jnp.arange(piece_len // key_span, dtype=jnp.int32))
    running_max, denominator, weighted = state_out
    heads_out = (weighted / denominator[:, :, None]).transpose(1, 0, 2).reshape(row_count, width)
    heads_out = heads_out.astype(jnp.bfloat16)
    token_count = moe_input.shape[0]
    top_count = routes.shape[1]
    local_experts = expert_gate.shape[0]
    ep_count = lax.axis_size("ep")
    expert_count = local_experts * ep_count
    capacity = 2 * token_count * top_count // expert_count
    column_count = expert_down.shape[2]
    first_column = lax.axis_index("tp") * column_count
    moe_rows = moe_input.astype(jnp.float32)
    normed = (
        moe_rows
        * lax.rsqrt(jnp.mean(moe_rows * moe_rows, axis=1, keepdims=True) + norm_eps)
        * moe_gain
    ).astype(jnp.bfloat16)
    flat_routes = routes.reshape(-1)
    one_hot = (flat_routes[:, None] == jnp.arange(expert_count, dtype=jnp.int32)[None, :]).astype(
        jnp.int32
    )
    ranks = jnp.sum(jnp.cumsum(one_hot, axis=0) * one_hot, axis=1) - 1
    slot_index = flat_routes * capacity + ranks
    pair_token = jnp.arange(token_count * top_count, dtype=jnp.int32) // top_count
    slot_token = (
        jnp.full((expert_count * capacity,), token_count, jnp.int32).at[slot_index].set(pair_token)
    )
    padded = jnp.concatenate([normed, jnp.zeros((1, normed.shape[1]), jnp.bfloat16)], axis=0)
    outgoing = lax.dynamic_slice_in_dim(padded, first_column, column_count, 1)[slot_token]
    outgoing = outgoing.reshape(ep_count, local_experts, capacity, outgoing.shape[1])
    arrived = lax.all_to_all(outgoing, "ep", split_axis=0, concat_axis=0, tiled=True)
    arrived = lax.all_gather(arrived, "tp", axis=3, tiled=True)
    gate_val = jnp.einsum(
        "aecd,edf->aecf", arrived, expert_gate, preferred_element_type=jnp.float32
    )
    up_val = jnp.einsum("aecd,edf->aecf", arrived, expert_up, preferred_element_type=jnp.float32)
    hidden = (jax.nn.silu(gate_val) * up_val).astype(jnp.bfloat16)
    hidden = collect(hidden, "tp", 3)
    result = jnp.einsum(
        "aecf,efd->aecd", hidden, expert_down, preferred_element_type=jnp.float32
    ).astype(jnp.bfloat16)
    returned = lax.all_to_all(result, "ep", split_axis=0, concat_axis=0, tiled=True)
    picked = returned.reshape(expert_count * capacity, column_count)[slot_index]
    picked = picked.astype(jnp.float32).reshape(token_count, top_count, column_count)
    routed = jnp.sum(picked * route_weight[:, :, None], axis=1)
    shared_hidden = (
        jax.nn.silu(jnp.dot(normed, shared_gate, preferred_element_type=jnp.float32))
        * jnp.dot(normed, shared_up, preferred_element_type=jnp.float32)
    ).astype(jnp.bfloat16)
    mixer_sum = jnp.dot(
        lax.all_gather(heads_out, "tp", axis=1, tiled=True),
        out_weight,
        preferred_element_type=jnp.float32,
    )
    shared_all = lax.all_gather(shared_hidden, "tp", axis=1, tiled=True)
    moe_total = routed + jnp.dot(shared_all, shared_down, preferred_element_type=jnp.float32)
    return (mixer_sum.astype(jnp.bfloat16), moe_total.astype(jnp.bfloat16))


def solution(mesh):
    placed = (
        P("ep", "tp"),
        P("ep", "tp"),
        P("ep", "tp"),
        P("tp", None),
        P(None, "tp"),
        P("ep", None),
        P(),
        P("ep", None),
        P("ep", None),
        P("ep", None, "tp"),
        P("ep", None, "tp"),
        P("ep", None, "tp"),
        P(None, "tp"),
        P(None, "tp"),
        P(None, "tp"),
    )
    return jax.shard_map(
        local, mesh=mesh, in_specs=placed, out_specs=(P("ep", "tp"), P("ep", "tp")), check_vma=False
    )
```

profile of v0, /device:TPU:1, one launch (start us, length us, event | category | flops | bytes accessed | tf_op | source)
XLA Modules:
  0.0 554.8 jit_solution(1330439696241112962)
XLA Ops:
  7.2 0.7 broadcast_multiply_fusion
  8.0 0.8 copy.43
  8.8 1.4 fusion.15
  11.6 4.1 scatter_custom_fusion
  16.0 2.9 gather_fusion
  19.3 40.2 %all_to_all.15 = bf16[32,4,9,128]{3,1,2,0:T(4,128)(2,1)S(1)} all-to-all(bf16[32,4,9,128]{3,1,2,0:T(4,128)(2,1)S(1)} %copy.46), channel_id=1, replica_groups=mesh['ep'=32,'tp'=16] {'ep'}, dimensions={0} | all-to-all | bytes 589824 | tf_op jit(solution)/shard_map/all_to_all | solution.py:128
  59.5 0.8 copy.47
  60.7 0.8 pad_maximum_fusion
  61.6 63.6 %all-gather.7.cloned.1.call-done = bf16[32,4,9,2048]{3,0,2,1:T(8,128)(2,1)} async-done(((bf16[32,4,9,128]{3,0,2,1:T(8,128)(2,1)}), bf16[32,4,9,2048]{3,0,2,1:T(8,128)(2,1)}) %all-gather.7.cloned.1.call-update) | async-done | bytes 4718608 | tf_op jit(solution)/shard_map/all_gather | solution.py:129
  125.2 3.8 convolution_bitcast_fusion.2
  129.1 1.4 fusion.21
  130.5 3.2 broadcast_bitcast_fusion
  133.7 7.8 %reshape.164 = bf16[16,2,18432]{2,1,0:T(2,128)(2,1)} reshape(bf16[16,4,9,32,32]{4,3,2,1,0:T(8,128)(2,1)} %broadcast_bitcast_fusion) | data formatting | bytes 2359296
  141.5 4.8 all-to-all-start.1
  146.6 0.7 constant_dynamic-slice_fusion.1
  147.2 58.1 %all-gather.5.cloned.1.call-done = bf16[24576,128]{1,0:T(8,128)(2,1)} async-done(((bf16[768,128]{1,0:T(8,128)(2,1)}), bf16[24576,128]{1,0:T(8,128)(2,1)}) %all-gather.5.cloned.1.call-update) | async-done | bytes 6291472 | tf_op jit(solution)/shard_map/all_gather | solution.py:58
  205.4 76.2 %while.15 = (s32[]{:T(128)}, f32[1,768]{1,0:T(1,128)S(1)}, f32[1,768]{1,0:T(1,128)S(1)}, f32[1,768,64]{1,2,0:T(8,128)S(1)}, s32[48]{0:T(128)S(1)}, /*index=5*/s3...) while((s32[]{:T(128)}, f32[1,768]{1,0:T(1,128)S(1)}, ...), condition=%wide.region_5.6_spmd.clone, body=%wide.region_0.5_spmd.clone.sunk | while | flops 106270224 | bytes 5566899 | solution.py:97
  205.4 0.6 dynamic_slice.23
  206.7 4.7 conditional.3
  207.4 0.8 constant_dynamic-slice_fusion
  208.1 1.4 fusion.40
  209.6 1.4 fusion.4
  212.6 4.7 conditional.3
  213.3 0.8 constant_dynamic-slice_fusion
  214.1 1.4 fusion.40
  215.5 1.4 fusion.4
  217.3 0.6 dynamic_slice.23
  218.6 4.7 conditional.3
  219.3 0.8 constant_dynamic-slice_fusion
  220.0 1.4 fusion.40
  221.5 1.4 fusion.4
  223.3 0.6 dynamic_slice.23
  224.6 0.6 dynamic_slice.23
  227.2 0.6 dynamic_slice.23
  228.5 0.6 dynamic_slice.23
  229.7 0.6 dynamic_slice.23
  231.0 0.6 dynamic_slice.23
  233.6 0.6 dynamic_slice.23
  234.9 0.6 dynamic_slice.23
  236.2 0.6 dynamic_slice.23
  237.5 0.6 dynamic_slice.23
  240.1 0.6 dynamic_slice.23
  241.4 0.6 dynamic_slice.23
  242.7 0.6 dynamic_slice.23
  245.3 0.6 dynamic_slice.23
  246.6 0.6 dynamic_slice.23
  247.9 0.6 dynamic_slice.23
  249.2 0.6 dynamic_slice.23
  251.8 0.6 dynamic_slice.23
  253.1 0.6 dynamic_slice.23
  254.4 0.6 dynamic_slice.23
  255.7 0.6 dynamic_slice.23
  281.6 0.7 divide_convert_fusion
  282.3 3.8 reshape.165
  286.1 3.1 bitcast_bitcast_fusion
  289.2 7.6 %copy.48 = bf16[32,4,9,16,32]{4,3,0,2,1:T(8,128)(2,1)} copy(bf16[32,4,9,16,32]{4,0,2,1,3:T(8,128)(2,1)S(1)} %bitcast_bitcast_fusion) | data formatting | bytes 2359296 | tf_op jit(solution)/shard_map/transpose | solution.py:14
  296.8 6.5 %reshape.124 = bf16[32,4,9,512]{3,0,2,1:T(8,128)(2,1)S(1)} reshape(bf16[32,4,9,16,32]{4,3,0,2,1:T(8,128)(2,1)} %copy.48) | data formatting | bytes 2359296 | tf_op jit(solution)/shard_map/reshape | solution.py:14
  303.8 0.9 copy.49
  304.7 213.7 %all-to-all-start.2 = ((bf16[32,4,9,128]{3,1,2,0:T(4,128)(2,1)}), bf16[32,4,9,128]{3,1,2,0:T(4,128)(2,1)S(1)}, u32[]{:S(2)}, u32[]{:S(2)}) async-start(bf16[32,4,9,128]{3,1,2,0:T(4,128)(2,1)} %copy.49), calls=%async_computation.2 | async-start | bytes 589824 | tf_op jit(solution)/shard_map/all_to_all | solution.py:139
  519.2 20.5 %all_gather.15 = bf16[192,512]{0,1:T(8,128)(2,1)S(1)} all-gather(bf16[192,32]{0,1:T(8,128)(2,1)S(1)} %fusion.27), channel_id=1, replica_groups=mesh['ep'=32,'tp'=16] {'tp'}, dimensions={1}, use_global_device_ids=true | all-gather | bytes 208896 | tf_op jit(solution)/shard_map/all_gather | solution.py:152
  539.7 2.2 all-to-all-done.2
  542.2 1.9 gather_fusion.1
  544.6 0.9 fusion.26
  545.5 2.7 fusion.22
  (212 shorter events, 21.4 us)
Async XLA Ops:
  7.2 296.1 %copy-start = (bf16[4,512,128]{2,1,0:T(8,128)(2,1)S(1)}, bf16[4,512,128]{2,1,0:T(8,128)(2,1)}, u32[]{:S(2)}) copy-start(bf16[4,512,128]{2,1,0:T(8,128)(2,1)} %param.30) | copy-start | bytes 1572868
  7.2 118.0 %all-gather.7.cloned.1.call-start = ((), (), s32[]{:S(2)}) async-start(), calls=%async_computation.4 | async-start | bytes 5013504 | tf_op jit(solution)/shard_map/all_gather | solution.py:129
  10.9 4.8 copy-start.1
  10.9 4.8 copy-start.8
  19.0 41.4 %copy-start.6 = (bf16[768,64]{0,1:T(8,128)(2,1)S(1)}, bf16[768,64]{0,1:T(8,128)(2,1)}, u32[]{:S(2)}) copy-start(bf16[768,64]{0,1:T(8,128)(2,1)} %param.20) | copy-start | bytes 294916
  19.0 41.6 %copy-start.7 = (bf16[768,64]{0,1:T(8,128)(2,1)S(1)}, bf16[768,64]{0,1:T(8,128)(2,1)}, u32[]{:S(2)}) copy-start(bf16[768,64]{0,1:T(8,128)(2,1)} %param.21) | copy-start | bytes 294916
  19.3 105.9 %copy-start.11 = (bf16[4,2048,32]{1,2,0:T(8,128)(2,1)S(1)}, bf16[4,2048,32]{1,2,0:T(8,128)(2,1)}, u32[]{:S(2)}) copy-start(bf16[4,2048,32]{1,2,0:T(8,128)(2,1)} %param.28) | copy-start | bytes 1572868
  60.3 145.0 %all-gather.5.cloned.1.call-start = ((), (), s32[]{:S(2)}) async-start(), calls=%async_computation.3 | async-start | bytes 6488064 | tf_op jit(solution)/shard_map/all_gather | solution.py:58
  61.6 67.5 %copy-start.12 = (bf16[4,2048,32]{1,2,0:T(8,128)(2,1)S(1)}, bf16[4,2048,32]{1,2,0:T(8,128)(2,1)}, u32[]{:S(2)}) copy-start(bf16[4,2048,32]{1,2,0:T(8,128)(2,1)} %param.29) | copy-start | bytes 1572868
  125.2 3.9 copy-start.10
  141.5 63.9 %copy-start.13 = (bf16[768,64]{0,1:T(8,128)(2,1)S(1)}, bf16[768,64]{0,1:T(8,128)(2,1)}, u32[]{:S(2)}) copy-start(bf16[768,64]{0,1:T(8,128)(2,1)} %param.19) | copy-start | bytes 294916
  141.5 140.8 %all-to-all-start.1 = ((bf16[16,2,18432]{2,1,0:T(2,128)(2,1)}), bf16[16,2,18432]{2,1,0:T(2,128)(2,1)S(1)}, u32[]{:S(2)}, u32[]{:S(2)}) async-start(bf16[16,2,18432]{2,1,0:T(2,128)(2,1)} %reshape.164), calls=%async_computation.1 | async-start | bytes 2359296 | tf_op jit(solution)/shard_map/all_to_all | solution.py:19
  146.3 399.2 %all-gather.9.cloned.1.call-start = ((), (), s32[]{:S(2)}) async-start(), calls=%async_computation.5 | async-start | bytes 1671168 | tf_op jit(solution)/shard_map/all_gather | solution.py:148
  303.3 215.1 %copy-start.9 = (f32[192,3]{0,1:T(4,128)S(1)}, f32[192,3]{0,1:T(4,128)}, u32[]{:S(2)}) copy-start(f32[192,3]{0,1:T(4,128)} %param.27) | copy-start | bytes 6916
  303.3 215.2 %copy-start.4 = (bf16[2048,32]{0,1:T(8,128)(2,1)S(1)}, bf16[2048,32]{0,1:T(8,128)(2,1)}, u32[]{:S(2)}) copy-start(bf16[2048,32]{0,1:T(8,128)(2,1)} %param.31) | copy-start | bytes 393220
  303.8 215.1 %copy-start.5 = (bf16[2048,32]{0,1:T(8,128)(2,1)S(1)}, bf16[2048,32]{0,1:T(8,128)(2,1)}, u32[]{:S(2)}) copy-start(bf16[2048,32]{0,1:T(8,128)(2,1)} %param.32) | copy-start | bytes 393220
  304.7 237.3 %all-to-all-start.2 = ((bf16[32,4,9,128]{3,1,2,0:T(4,128)(2,1)}), bf16[32,4,9,128]{3,1,2,0:T(4,128)(2,1)S(1)}, u32[]{:S(2)}, u32[]{:S(2)}) async-start(bf16[32,4,9,128]{3,1,2,0:T(4,128)(2,1)} %copy.49), calls=%async_computation.2 | async-start | bytes 589824 | tf_op jit(solution)/shard_map/all_to_all | solution.py:139
  542.1 2.6 copy-start.3
  542.2 3.3 copy-start.2
Sparse Core Ops, SparseCore 0:
  60.4 64.7 all-gather.6
  127.9 77.4 all-gather.4
  282.4 260.1 all-gather.8
where the time goes:
time: 559 us; the launch traced here: 555 us
  starting transfers between devices  219 us (39%)
  waiting for transfers between devices  124 us (22%)
  local copies, waits for them, and re-layouts  76.5 us (14%)
  blocking collectives  60.7 us (11%)
  loops' own time  36.1 us (6%)
  matrix products  18.3 us (3%)
  between operations  14.2 us (3%)
  other arithmetic  6.13 us (1%)
    all_to_all x1, starting transfers between devices, local(): lax.all_to_all(result, 'ep', split_axis=0, concat_axis=0, tiled=True)  214 us
    all_gather x1, waiting for transfers between devices, local(): arrived = lax.all_gather(arrived, 'tp', axis=3, tiled=True)  63.6 us
    all_gather x1, waiting for transfers between devices, local(): shard_rows = lax.all_gather(key_value, 'ep', axis=0, tiled=True)  58.1 us
    all_to_all x1, blocking collectives, local(): lax.all_to_all(outgoing, 'ep', split_axis=0, concat_axis=0, tiled=True)  40.2 us
    another operation x1, loops' own time, local(): lax.scan(one_span, initial, jnp.arange(piece_len // key_span, dtype=jnp.i...  33.2 us
    dynamic_slice x48, local copies, waits for them, and re-layouts, local(): lax.scan(one_span, initial, jnp.arange(piece_len // key_span, dtype=jnp.i...  28.1 us
    all_gather x1, blocking collectives, local(): shared_all = lax.all_gather(shared_hidden, 'tp', axis=1, tiled=True)  20.5 us
    unnamed x35, local copies, waits for them, and re-layouts  16.1 us
  transfers between devices with their start and end apart: 5, of which 3 were waited for; matrix products, arithmetic and copies ran while one was open for 15% of the time, Pallas kernels for 0%

commit v1 on v0

--- a/solution.py
+++ b/solution.py
@@ -6,6 +6,27 @@
 HEAD = 64
 neg_fill = -1e30
 norm_eps = 1e-06
+
+
+def collect_2(x, axis, dim):
+    size, index, rows = (lax.axis_size(axis), lax.axis_index(axis), x.shape[dim])
+    upward = [(i, (i + 1) % size) for i in range(size)]
+    left = [(i, (i - 1) % size) for i in range(size)]
+    filled = jnp.zeros((*x.shape[:dim], size * rows, *x.shape[dim + 1 :]), x.dtype)
+    filled = lax.dynamic_update_slice_in_dim(filled, x, index * rows, axis=dim)
+    from_left = from_right = x
+    middle = size // 2
+    for hop in range(1, middle + 1):
+        from_left = lax.ppermute(from_left, axis, upward)
+        filled = lax.dynamic_update_slice_in_dim(
+            filled, from_left, (index - hop) % size * rows, axis=dim
+        )
+        if hop < size - middle:
+            from_right = lax.ppermute(from_right, axis, left)
+            filled = lax.dynamic_update_slice_in_dim(
+                filled, from_right, (index + hop) % size * rows, axis=dim
+            )
+    return filled
 
 
 def joined_along(pieces, dim):
@@ -126,7 +147,7 @@
     outgoing = lax.dynamic_slice_in_dim(padded, first_column, column_count, 1)[slot_token]
     outgoing = outgoing.reshape(ep_count, local_experts, capacity, outgoing.shape[1])
     arrived = lax.all_to_all(outgoing, "ep", split_axis=0, concat_axis=0, tiled=True)
-    arrived = lax.all_gather(arrived, "tp", axis=3, tiled=True)
+    arrived = collect_2(arrived, "tp", 3)
     gate_val = jnp.einsum(
         "aecd,edf->aecf", arrived, expert_gate, preferred_element_type=jnp.float32
     )

time: 559 us -> 531 us (0.950)
  waiting for transfers between devices: 124 us -> 26.1 us
  starting transfers between devices: 219 us -> 282 us
  local copies, waits for them, and re-layouts: 76.5 us -> 83.2 us
    all_gather x1 -> x0, waiting for transfers between devices: 63.6 us -> none  [local(): arrived = lax.all_gather(arrived, 'tp', axis=3, tiled=True)]
    ppermute x0 -> x15, starting transfers between devices: none -> 62.4 us  [the longest x7 45.8 us: collect_2(): from_right = lax.ppermute(from_right, axis, left)]
    all_gather x1, waiting for transfers between devices: 58.1 us -> 0.01 us  [local(): shard_rows = lax.all_gather(key_value, 'ep', axis=0, tiled=True)]
    ppermute x0 -> x15, waiting for transfers between devices: none -> 24.2 us  [the longest x8 24.2 us: collect_2(): from_left = lax.ppermute(from_left, axis, upward)]
    unnamed x35 -> x31, local copies, waits for them, and re-layouts: 16.1 us -> 21.1 us
  transfers between devices with their start and end apart: 5 -> 19, of which waited for: 3 -> 9; matrix products, arithmetic and copies ran while one was open for 15% -> 19% of each run, Pallas kernels for 0% -> 0%
where the time goes in v1:
time: 531 us; the launch traced here: 526 us
  starting transfers between devices  282 us (53%)
  local copies, waits for them, and re-layouts  83.2 us (16%)
  blocking collectives  63.1 us (12%)
  loops' own time  35.9 us (7%)
  waiting for transfers between devices  26.1 us (5%)
  matrix products  15.8 us (3%)
  between operations  15.1 us (3%)
    all_to_all x1, starting transfers between devices, local(): lax.all_to_all(result, 'ep', split_axis=0, concat_axis=0, tiled=True)  215 us
    ppermute x7, starting transfers between devices, collect_2(): from_right = lax.ppermute(from_right, axis, left)  45.8 us
    all_to_all x1, blocking collectives, local(): lax.all_to_all(outgoing, 'ep', split_axis=0, concat_axis=0, tiled=True)  42.2 us
    another operation x1, loops' own time, local(): lax.scan(one_span, initial, jnp.arange(piece_len // key_span, dtype=jnp.i...  33.1 us
    dynamic_slice x48, local copies, waits for them, and re-layouts, local(): lax.scan(one_span, initial, jnp.arange(piece_len // key_span, dtype=jnp.i...  28.2 us
    ppermute x8, waiting for transfers between devices, collect_2(): from_left = lax.ppermute(from_left, axis, upward)  24.2 us
    unnamed x31, local copies, waits for them, and re-layouts  21.1 us
    all_gather x1, blocking collectives, local(): shared_all = lax.all_gather(shared_hidden, 'tp', axis=1, tiled=True)  20.9 us
  transfers between devices with their start and end apart: 19, of which 9 were waited for; matrix products, arithmetic and copies ran while one was open for 19% of the time, Pallas kernels for 0%

profile of v1, /device:TPU:1, one launch (start us, length us, event | category | flops | bytes accessed | tf_op | source)
XLA Modules:
  0.0 525.8 jit_solution(16659211299161667795)
XLA Ops:
  7.3 1.1 copy.72
  8.4 1.1 copy.73
  9.5 0.8 pad_maximum_fusion
  10.3 0.8 copy.75
  12.5 4.1 scatter_custom_fusion
  17.2 2.9 gather_fusion
  20.4 42.2 %all_to_all.15 = bf16[32,4,9,128]{3,1,2,0:T(4,128)(2,1)S(1)} all-to-all(bf16[32,4,9,128]{3,1,2,0:T(4,128)(2,1)S(1)} %copy.78), channel_id=1, replica_groups=mesh['ep'=32,'tp'=16] {'ep'}, dimensions={0} | all-to-all | bytes 589824 | tf_op jit(solution)/shard_map/all_to_all | solution.py:149
  62.6 3.0 collective-permute-start
  65.7 5.7 %collective-permute-start.1 = (bf16[32,4,9,128]{3,1,2,0:T(4,128)(2,1)S(1)}, bf16[32,4,9,128]{3,1,2,0:T(4,128)(2,1)S(1)}, u32[]{:S(2)}, u32[]{:S(2)}) collective-permute-start(bf16[32,4,9,128]{3,1,2,0:T(4,128)(2,1)S(1)} %all_to_all.15), channel_id=1, source_target_pairs={{0,15},{1,0},{2,1},{3,2},{4,3},{5,4},{6,5},{7,6},{8,7},{9,8},{10,9... | collective-permute-start | bytes 884744 | tf_op jit(solution)/shard_map/ppermute | solution.py:25
  72.4 3.1 collective-permute-done
  75.5 1.9 collective-permute-start.2
  77.4 6.7 %collective-permute-start.3 = (bf16[32,4,9,128]{3,1,2,0:T(4,128)(2,1)S(1)}, bf16[32,4,9,128]{3,1,2,0:T(4,128)(2,1)S(1)}, u32[]{:S(2)}, u32[]{:S(2)}) collective-permute-start(bf16[32,4,9,128]{3,1,2,0:T(4,128)(2,1)S(1)} %collective-permute-done.1), channel_id=1, source_target_pairs={{0,15},{1,0},{2,1},{3,2},{4,3},{5,4},{6,5},{7,6},{8,7},{9,8},{10,9... | collective-permute-start | bytes 884744 | tf_op jit(solution)/shard_map/ppermute | solution.py:25
  84.3 3.0 collective-permute-done.2
  87.3 1.9 collective-permute-start.4
  89.2 6.7 %collective-permute-start.5 = (bf16[32,4,9,128]{3,1,2,0:T(4,128)(2,1)S(1)}, bf16[32,4,9,128]{3,1,2,0:T(4,128)(2,1)S(1)}, u32[]{:S(2)}, u32[]{:S(2)}) collective-permute-start(bf16[32,4,9,128]{3,1,2,0:T(4,128)(2,1)S(1)} %collective-permute-done.3), channel_id=1, source_target_pairs={{0,15},{1,0},{2,1},{3,2},{4,3},{5,4},{6,5},{7,6},{8,7},{9,8},{10,9... | collective-permute-start | bytes 884744 | tf_op jit(solution)/shard_map/ppermute | solution.py:25
  96.2 1.9 collective-permute-done.4
  98.1 1.9 collective-permute-start.6
  100.0 6.7 %collective-permute-start.7 = (bf16[32,4,9,128]{3,1,2,0:T(4,128)(2,1)S(1)}, bf16[32,4,9,128]{3,1,2,0:T(4,128)(2,1)S(1)}, u32[]{:S(2)}, u32[]{:S(2)}) collective-permute-start(bf16[32,4,9,128]{3,1,2,0:T(4,128)(2,1)S(1)} %collective-permute-done.5), channel_id=1, source_target_pairs={{0,15},{1,0},{2,1},{3,2},{4,3},{5,4},{6,5},{7,6},{8,7},{9,8},{10,9... | collective-permute-start | bytes 884744 | tf_op jit(solution)/shard_map/ppermute | solution.py:25
  106.9 1.9 collective-permute-done.6
  108.9 1.9 collective-permute-start.8
  110.8 6.7 %collective-permute-start.9 = (bf16[32,4,9,128]{3,1,2,0:T(4,128)(2,1)S(1)}, bf16[32,4,9,128]{3,1,2,0:T(4,128)(2,1)S(1)}, u32[]{:S(2)}, u32[]{:S(2)}) collective-permute-start(bf16[32,4,9,128]{3,1,2,0:T(4,128)(2,1)S(1)} %collective-permute-done.7), channel_id=1, source_target_pairs={{0,15},{1,0},{2,1},{3,2},{4,3},{5,4},{6,5},{7,6},{8,7},{9,8},{10,9... | collective-permute-start | bytes 884744 | tf_op jit(solution)/shard_map/ppermute | solution.py:25
  117.7 1.9 collective-permute-done.8
  119.6 1.9 collective-permute-start.10
  121.6 6.7 %collective-permute-start.11 = (bf16[32,4,9,128]{3,1,2,0:T(4,128)(2,1)S(1)}, bf16[32,4,9,128]{3,1,2,0:T(4,128)(2,1)S(1)}, u32[]{:S(2)}, u32[]{:S(2)}) collective-permute-start(bf16[32,4,9,128]{3,1,2,0:T(4,128)(2,1)S(1)} %collective-permute-done.9), channel_id=1, source_target_pairs={{0,15},{1,0},{2,1},{3,2},{4,3},{5,4},{6,5},{7,6},{8,7},{9,8},{10,9... | collective-permute-start | bytes 884744 | tf_op jit(solution)/shard_map/ppermute | solution.py:25
  128.5 1.9 collective-permute-done.10
  130.4 1.9 collective-permute-start.12
  132.3 6.7 %collective-permute-start.13 = (bf16[32,4,9,128]{3,1,2,0:T(4,128)(2,1)S(1)}, bf16[32,4,9,128]{3,1,2,0:T(4,128)(2,1)S(1)}, u32[]{:S(2)}, u32[]{:S(2)}) collective-permute-start(bf16[32,4,9,128]{3,1,2,0:T(4,128)(2,1)S(1)} %collective-permute-done.11), channel_id=1, source_target_pairs={{0,15},{1,0},{2,1},{3,2},{4,3},{5,4},{6,5},{7,6},{8,7},{9,8},{10,9... | collective-permute-start | bytes 884744 | tf_op jit(solution)/shard_map/ppermute | solution.py:25
  139.3 1.9 collective-permute-done.12
  141.2 2.1 collective-permute-start.14
  143.5 8.7 %collective-permute-done.14 = bf16[32,4,9,128]{3,1,2,0:T(4,128)(2,1)S(1)} collective-permute-done((bf16[32,4,9,128]{3,1,2,0:T(4,128)(2,1)S(1)}, bf16[32,4,9,128]{3,1,2,0:T(4,128)(2,1)S(1)}, u32[]{:S(2)}, u32[]{:S(2)}) %collective-permute-start.14) | collective-permute-done | bytes 294944 | tf_op jit(solution)/shard_map/ppermute | solution.py:20
  152.3 1.4 convolution_bitcast_fusion.2
  153.7 1.4 multiply_convert_fusion
  155.1 3.2 broadcast_bitcast_fusion
  158.3 7.9 %reshape.164 = bf16[16,2,18432]{2,1,0:T(2,128)(2,1)} reshape(bf16[16,4,9,32,32]{4,3,2,1,0:T(8,128)(2,1)} %broadcast_bitcast_fusion) | data formatting | bytes 2359296
  166.2 4.4 all-to-all-start.1
  170.6 0.7 constant_dynamic-slice_fusion.1
  171.4 76.1 %while.15 = (s32[]{:T(128)}, f32[1,768]{1,0:T(1,128)S(1)}, f32[1,768]{1,0:T(1,128)S(1)}, f32[1,768,64]{1,2,0:T(8,128)S(1)}, s32[48]{0:T(128)S(1)}, /*index=5*/s3...) while((s32[]{:T(128)}, f32[1,768]{1,0:T(1,128)S(1)}, ...), condition=%wide.region_5.6_spmd.clone, body=%wide.region_0.5_spmd.clone.sunk | while | flops 106270224 | bytes 5566891 | solution.py:118
  172.6 4.7 conditional.3
  172.7 0.8 constant_dynamic-slice_fusion
  174.1 1.4 fusion.40
  175.5 1.4 fusion.4
  178.6 4.7 conditional.3
  178.6 0.8 constant_dynamic-slice_fusion
  180.1 1.4 fusion.40
  181.5 1.4 fusion.4
  184.6 4.7 conditional.3
  184.6 0.8 constant_dynamic-slice_fusion
  186.1 1.4 fusion.40
  187.5 1.4 fusion.4
  193.2 0.6 dynamic_slice.23
  202.2 0.6 dynamic_slice.23
  217.7 0.6 dynamic_slice.23
  247.5 0.7 divide_convert_fusion
  248.2 6.9 %reshape.165 = bf16[16,4,9,32,32]{4,3,2,1,0:T(8,128)(2,1)} reshape(bf16[16,2,18432]{2,1,0:T(2,128)(2,1)} %all-to-all-done.1) | data formatting | bytes 2359296
  255.0 3.1 bitcast_bitcast_fusion
  258.2 7.6 %copy.95 = bf16[32,4,9,16,32]{4,3,0,2,1:T(8,128)(2,1)} copy(bf16[32,4,9,16,32]{4,0,2,1,3:T(8,128)(2,1)S(1)} %bitcast_bitcast_fusion) | data formatting | bytes 2359296 | tf_op jit(solution)/shard_map/transpose | solution.py:35
  265.8 6.5 %reshape.124 = bf16[32,4,9,512]{3,0,2,1:T(8,128)(2,1)S(1)} reshape(bf16[32,4,9,16,32]{4,3,0,2,1:T(8,128)(2,1)} %copy.95) | data formatting | bytes 2359296 | tf_op jit(solution)/shard_map/reshape | solution.py:35
  272.8 0.9 copy.96
  273.7 215.4 %all-to-all-start.2 = ((bf16[32,4,9,128]{3,1,2,0:T(4,128)(2,1)}), bf16[32,4,9,128]{3,1,2,0:T(4,128)(2,1)S(1)}, u32[]{:S(2)}, u32[]{:S(2)}) async-start(bf16[32,4,9,128]{3,1,2,0:T(4,128)(2,1)} %copy.96), calls=%async_computation.2 | async-start | bytes 589824 | tf_op jit(solution)/shard_map/all_to_all | solution.py:160
  490.0 20.9 %all_gather.11 = bf16[192,512]{0,1:T(8,128)(2,1)S(1)} all-gather(bf16[192,32]{0,1:T(8,128)(2,1)S(1)} %fusion.25), channel_id=1, replica_groups=mesh['ep'=32,'tp'=16] {'tp'}, dimensions={1}, use_global_device_ids=true | all-gather | bytes 208896 | tf_op jit(solution)/shard_map/all_gather | solution.py:173
  510.9 1.8 all-to-all-done.2
  513.0 1.9 gather_fusion.1
  515.4 0.9 fusion.24
  516.3 2.7 fusion.20
  (251 shorter events, 35.1 us)
Async XLA Ops:
  7.2 265.1 %copy-start = (bf16[4,512,128]{2,1,0:T(8,128)(2,1)S(1)}, bf16[4,512,128]{2,1,0:T(8,128)(2,1)}, u32[]{:S(2)}) copy-start(bf16[4,512,128]{2,1,0:T(8,128)(2,1)} %param.30) | copy-start | bytes 1572868
  7.2 4.7 copy-start.6
  7.2 9.5 %copy-start.1 = (bf16[192,2048]{1,0:T(8,128)(2,1)S(1)}, bf16[192,2048]{1,0:T(8,128)(2,1)}, u32[]{:S(2)}) copy-start(bf16[192,2048]{1,0:T(8,128)(2,1)} %param.24) | copy-start | bytes 2359300
  7.2 9.7 %copy-start.7 = (f32[2048]{0:T(1024)S(1)}, f32[2048]{0:T(1024)}, u32[]{:S(2)}) copy-start(f32[2048]{0:T(1024)} %param.25) | copy-start | bytes 24580
  7.2 164.1 %all-gather.4.cloned.1.call-start = ((), (), s32[]{:S(2)}) async-start(), calls=%async_computation.3 | async-start | bytes 6488064 | tf_op jit(solution)/shard_map/all_gather | solution.py:79
  62.6 12.8 %collective-permute-start = (bf16[32,4,9,128]{3,1,2,0:T(4,128)(2,1)S(1)}, bf16[32,4,9,128]{3,1,2,0:T(4,128)(2,1)S(1)}, u32[]{:S(2)}, u32[]{:S(2)}) collective-permute-start(bf16[32,4,9,128]{3,1,2,0:T(4,128)(2,1)S(1)} %all_to_all.15), channel_id=1, source_target_pairs={{0,1},{1,2},{2,3},{3,4},{4,5},{5,6},{6,7},{7,8},{8,9},{9,10},{10,1... | collective-permute-start | bytes 884744 | tf_op jit(solution)/shard_map/ppermute | solution.py:20
  65.7 11.7 %collective-permute-start.1 = (bf16[32,4,9,128]{3,1,2,0:T(4,128)(2,1)S(1)}, bf16[32,4,9,128]{3,1,2,0:T(4,128)(2,1)S(1)}, u32[]{:S(2)}, u32[]{:S(2)}) collective-permute-start(bf16[32,4,9,128]{3,1,2,0:T(4,128)(2,1)S(1)} %all_to_all.15), channel_id=1, source_target_pairs={{0,15},{1,0},{2,1},{3,2},{4,3},{5,4},{6,5},{7,6},{8,7},{9,8},{10,9... | collective-permute-start | bytes 884744 | tf_op jit(solution)/shard_map/ppermute | solution.py:25
  72.3 80.0 %copy-start.9 = (bf16[4,2048,32]{1,2,0:T(8,128)(2,1)S(1)}, bf16[4,2048,32]{1,2,0:T(8,128)(2,1)}, u32[]{:S(2)}) copy-start(bf16[4,2048,32]{1,2,0:T(8,128)(2,1)} %param.28) | copy-start | bytes 1572868
  75.5 11.8 %collective-permute-start.2 = (bf16[32,4,9,128]{3,1,2,0:T(4,128)(2,1)S(1)}, bf16[32,4,9,128]{3,1,2,0:T(4,128)(2,1)S(1)}, u32[]{:S(2)}, u32[]{:S(2)}) collective-permute-start(bf16[32,4,9,128]{3,1,2,0:T(4,128)(2,1)S(1)} %collective-permute-done), channel_id=1, source_target_pairs={{0,1},{1,2},{2,3},{3,4},{4,5},{5,6},{6,7},{7,8},{8,9},{9,10},{10,1... | collective-permute-start | bytes 884744 | tf_op jit(solution)/shard_map/ppermute | solution.py:20
  77.4 11.8 %collective-permute-start.3 = (bf16[32,4,9,128]{3,1,2,0:T(4,128)(2,1)S(1)}, bf16[32,4,9,128]{3,1,2,0:T(4,128)(2,1)S(1)}, u32[]{:S(2)}, u32[]{:S(2)}) collective-permute-start(bf16[32,4,9,128]{3,1,2,0:T(4,128)(2,1)S(1)} %collective-permute-done.1), channel_id=1, source_target_pairs={{0,15},{1,0},{2,1},{3,2},{4,3},{5,4},{6,5},{7,6},{8,7},{9,8},{10,9... | collective-permute-start | bytes 884744 | tf_op jit(solution)/shard_map/ppermute | solution.py:25
  87.3 10.8 %collective-permute-start.4 = (bf16[32,4,9,128]{3,1,2,0:T(4,128)(2,1)S(1)}, bf16[32,4,9,128]{3,1,2,0:T(4,128)(2,1)S(1)}, u32[]{:S(2)}, u32[]{:S(2)}) collective-permute-start(bf16[32,4,9,128]{3,1,2,0:T(4,128)(2,1)S(1)} %collective-permute-done.2), channel_id=1, source_target_pairs={{0,1},{1,2},{2,3},{3,4},{4,5},{5,6},{6,7},{7,8},{8,9},{9,10},{10,1... | collective-permute-start | bytes 884744 | tf_op jit(solution)/shard_map/ppermute | solution.py:20
  89.2 10.8 %collective-permute-start.5 = (bf16[32,4,9,128]{3,1,2,0:T(4,128)(2,1)S(1)}, bf16[32,4,9,128]{3,1,2,0:T(4,128)(2,1)S(1)}, u32[]{:S(2)}, u32[]{:S(2)}) collective-permute-start(bf16[32,4,9,128]{3,1,2,0:T(4,128)(2,1)S(1)} %collective-permute-done.3), channel_id=1, source_target_pairs={{0,15},{1,0},{2,1},{3,2},{4,3},{5,4},{6,5},{7,6},{8,7},{9,8},{10,9... | collective-permute-start | bytes 884744 | tf_op jit(solution)/shard_map/ppermute | solution.py:25
  98.1 10.8 %collective-permute-start.6 = (bf16[32,4,9,128]{3,1,2,0:T(4,128)(2,1)S(1)}, bf16[32,4,9,128]{3,1,2,0:T(4,128)(2,1)S(1)}, u32[]{:S(2)}, u32[]{:S(2)}) collective-permute-start(bf16[32,4,9,128]{3,1,2,0:T(4,128)(2,1)S(1)} %collective-permute-done.4), channel_id=1, source_target_pairs={{0,1},{1,2},{2,3},{3,4},{4,5},{5,6},{6,7},{7,8},{8,9},{9,10},{10,1... | collective-permute-start | bytes 884744 | tf_op jit(solution)/shard_map/ppermute | solution.py:20
  100.0 10.8 %collective-permute-start.7 = (bf16[32,4,9,128]{3,1,2,0:T(4,128)(2,1)S(1)}, bf16[32,4,9,128]{3,1,2,0:T(4,128)(2,1)S(1)}, u32[]{:S(2)}, u32[]{:S(2)}) collective-permute-start(bf16[32,4,9,128]{3,1,2,0:T(4,128)(2,1)S(1)} %collective-permute-done.5), channel_id=1, source_target_pairs={{0,15},{1,0},{2,1},{3,2},{4,3},{5,4},{6,5},{7,6},{8,7},{9,8},{10,9... | collective-permute-start | bytes 884744 | tf_op jit(solution)/shard_map/ppermute | solution.py:25
  108.9 10.8 %collective-permute-start.8 = (bf16[32,4,9,128]{3,1,2,0:T(4,128)(2,1)S(1)}, bf16[32,4,9,128]{3,1,2,0:T(4,128)(2,1)S(1)}, u32[]{:S(2)}, u32[]{:S(2)}) collective-permute-start(bf16[32,4,9,128]{3,1,2,0:T(4,128)(2,1)S(1)} %collective-permute-done.6), channel_id=1, source_target_pairs={{0,1},{1,2},{2,3},{3,4},{4,5},{5,6},{6,7},{7,8},{8,9},{9,10},{10,1... | collective-permute-start | bytes 884744 | tf_op jit(solution)/shard_map/ppermute | solution.py:20
  110.8 10.8 %collective-permute-start.9 = (bf16[32,4,9,128]{3,1,2,0:T(4,128)(2,1)S(1)}, bf16[32,4,9,128]{3,1,2,0:T(4,128)(2,1)S(1)}, u32[]{:S(2)}, u32[]{:S(2)}) collective-permute-start(bf16[32,4,9,128]{3,1,2,0:T(4,128)(2,1)S(1)} %collective-permute-done.7), channel_id=1, source_target_pairs={{0,15},{1,0},{2,1},{3,2},{4,3},{5,4},{6,5},{7,6},{8,7},{9,8},{10,9... | collective-permute-start | bytes 884744 | tf_op jit(solution)/shard_map/ppermute | solution.py:25
  119.6 10.8 %collective-permute-start.10 = (bf16[32,4,9,128]{3,1,2,0:T(4,128)(2,1)S(1)}, bf16[32,4,9,128]{3,1,2,0:T(4,128)(2,1)S(1)}, u32[]{:S(2)}, u32[]{:S(2)}) collective-permute-start(bf16[32,4,9,128]{3,1,2,0:T(4,128)(2,1)S(1)} %collective-permute-done.8), channel_id=1, source_target_pairs={{0,1},{1,2},{2,3},{3,4},{4,5},{5,6},{6,7},{7,8},{8,9},{9,10},{10,1... | collective-permute-start | bytes 884744 | tf_op jit(solution)/shard_map/ppermute | solution.py:20
  121.6 10.8 %collective-permute-start.11 = (bf16[32,4,9,128]{3,1,2,0:T(4,128)(2,1)S(1)}, bf16[32,4,9,128]{3,1,2,0:T(4,128)(2,1)S(1)}, u32[]{:S(2)}, u32[]{:S(2)}) collective-permute-start(bf16[32,4,9,128]{3,1,2,0:T(4,128)(2,1)S(1)} %collective-permute-done.9), channel_id=1, source_target_pairs={{0,15},{1,0},{2,1},{3,2},{4,3},{5,4},{6,5},{7,6},{8,7},{9,8},{10,9... | collective-permute-start | bytes 884744 | tf_op jit(solution)/shard_map/ppermute | solution.py:25
  130.4 10.8 %collective-permute-start.12 = (bf16[32,4,9,128]{3,1,2,0:T(4,128)(2,1)S(1)}, bf16[32,4,9,128]{3,1,2,0:T(4,128)(2,1)S(1)}, u32[]{:S(2)}, u32[]{:S(2)}) collective-permute-start(bf16[32,4,9,128]{3,1,2,0:T(4,128)(2,1)S(1)} %collective-permute-done.10), channel_id=1, source_target_pairs={{0,1},{1,2},{2,3},{3,4},{4,5},{5,6},{6,7},{7,8},{8,9},{9,10},{10,1... | collective-permute-start | bytes 884744 | tf_op jit(solution)/shard_map/ppermute | solution.py:20
  132.3 11.1 %collective-permute-start.13 = (bf16[32,4,9,128]{3,1,2,0:T(4,128)(2,1)S(1)}, bf16[32,4,9,128]{3,1,2,0:T(4,128)(2,1)S(1)}, u32[]{:S(2)}, u32[]{:S(2)}) collective-permute-start(bf16[32,4,9,128]{3,1,2,0:T(4,128)(2,1)S(1)} %collective-permute-done.11), channel_id=1, source_target_pairs={{0,15},{1,0},{2,1},{3,2},{4,3},{5,4},{6,5},{7,6},{8,7},{9,8},{10,9... | collective-permute-start | bytes 884744 | tf_op jit(solution)/shard_map/ppermute | solution.py:25
  141.2 11.0 %collective-permute-start.14 = (bf16[32,4,9,128]{3,1,2,0:T(4,128)(2,1)S(1)}, bf16[32,4,9,128]{3,1,2,0:T(4,128)(2,1)S(1)}, u32[]{:S(2)}, u32[]{:S(2)}) collective-permute-start(bf16[32,4,9,128]{3,1,2,0:T(4,128)(2,1)S(1)} %collective-permute-done.12), channel_id=1, source_target_pairs={{0,1},{1,2},{2,3},{3,4},{4,5},{5,6},{6,7},{7,8},{8,9},{9,10},{10,1... | collective-permute-start | bytes 884744 | tf_op jit(solution)/shard_map/ppermute | solution.py:20
  152.3 1.4 copy-start.10
  158.3 13.1 %copy-start.11 = (bf16[768,64]{0,1:T(8,128)(2,1)S(1)}, bf16[768,64]{0,1:T(8,128)(2,1)}, u32[]{:S(2)}) copy-start(bf16[768,64]{0,1:T(8,128)(2,1)} %param.19) | copy-start | bytes 294916
  166.2 82.0 %all-to-all-start.1 = ((bf16[16,2,18432]{2,1,0:T(2,128)(2,1)}), bf16[16,2,18432]{2,1,0:T(2,128)(2,1)}, u32[]{:S(2)}, u32[]{:S(2)}) async-start(bf16[16,2,18432]{2,1,0:T(2,128)(2,1)} %reshape.164), calls=%async_computation.1 | async-start | bytes 2359296 | tf_op jit(solution)/shard_map/all_to_all | solution.py:40
  170.6 345.7 %all-gather.6.cloned.1.call-start = ((), (), s32[]{:S(2)}) async-start(), calls=%async_computation.4 | async-start | bytes 1671168 | tf_op jit(solution)/shard_map/all_gather | solution.py:169
  265.8 223.3 %copy-start.8 = (f32[192,3]{0,1:T(4,128)S(1)}, f32[192,3]{0,1:T(4,128)}, u32[]{:S(2)}) copy-start(f32[192,3]{0,1:T(4,128)} %param.27) | copy-start | bytes 6916
  265.8 223.5 %copy-start.4 = (bf16[2048,32]{0,1:T(8,128)(2,1)S(1)}, bf16[2048,32]{0,1:T(8,128)(2,1)}, u32[]{:S(2)}) copy-start(bf16[2048,32]{0,1:T(8,128)(2,1)} %param.31) | copy-start | bytes 393220
  265.8 223.8 %copy-start.5 = (bf16[2048,32]{0,1:T(8,128)(2,1)S(1)}, bf16[2048,32]{0,1:T(8,128)(2,1)}, u32[]{:S(2)}) copy-start(bf16[2048,32]{0,1:T(8,128)(2,1)} %param.32) | copy-start | bytes 393220
  272.3 243.1 %copy-start.3 = (bf16[512,128]{1,0:T(8,128)(2,1)S(1)}, bf16[512,128]{1,0:T(8,128)(2,1)}, u32[]{:S(2)}) copy-start(bf16[512,128]{1,0:T(8,128)(2,1)} %param.33) | copy-start | bytes 393220
  272.3 243.9 %copy-start.2 = (bf16[1024,128]{1,0:T(8,128)(2,1)S(1)}, bf16[1024,128]{1,0:T(8,128)(2,1)}, u32[]{:S(2)}) copy-start(bf16[1024,128]{1,0:T(8,128)(2,1)} %param.23) | copy-start | bytes 786436
  273.7 239.0 %all-to-all-start.2 = ((bf16[32,4,9,128]{3,1,2,0:T(4,128)(2,1)}), bf16[32,4,9,128]{3,1,2,0:T(4,128)(2,1)S(1)}, u32[]{:S(2)}, u32[]{:S(2)}) async-start(bf16[32,4,9,128]{3,1,2,0:T(4,128)(2,1)} %copy.96), calls=%async_computation.2 | async-start | bytes 589824 | tf_op jit(solution)/shard_map/all_to_all | solution.py:160
Sparse Core Ops, SparseCore 0:
  10.7 92.1 all-gather.3
  248.3 262.0 all-gather.5
